TPU v7x, 512 devices: a whole 4x4x16 slice. The times are simulated.
512 devices in a mesh: sp: 128 (over z, x, core), tp: 4 (over y).
Axes of the slice: x: 4, y: 4, z: 16, core: 2. Of those that a mesh axis runs over, the one named last changes fastest.
Arguments:
- tokens: bfloat16 [16384, 2048], P('sp', 'tp'), may hold values from -6 to 6
- conv_value_weight: bfloat16 [2048, 1024], P('sp', 'tp'), may hold values from -0.125 to 0.125
- conv_gate_weight: bfloat16 [2048, 1024], P('sp', 'tp'), may hold values from -0.125 to 0.125
- conv_kernel: bfloat16 [31, 1024], P(None, 'tp'), may hold values from -16 to 16
- conv_norm_gain: float32 [1024], P('tp'), may hold values from 0.1 to 1.9
- query_weight: bfloat16 [2048, 2048], P('sp', 'tp'), may hold values from -0.125 to 0.125
- key_weight: bfloat16 [2048, 2048], P('sp', 'tp'), may hold values from -0.125 to 0.125
- value_weight: bfloat16 [2048, 2048], P('sp', 'tp'), may hold values from -0.125 to 0.125
- input_gate_weight: bfloat16 [2048, 8], P(None, 'tp'), may hold values from -0.125 to 0.125
- forget_gate_weight: bfloat16 [2048, 8], P(None, 'tp'), may hold values from -0.125 to 0.125
- input_offset: float32 [16384, 8], P('sp', 'tp'), may hold values from -4 to 210
- forget_offset: float32 [16384, 8], P('sp', 'tp'), may hold values from 0 to 30
- memory_norm_gain: float32 [2048], P('tp'), may hold values from 0.1 to 1.9
- conv_out_weight: bfloat16 [1024, 2048], P('tp', 'sp'), may hold values from -0.3125 to 0.3125
- memory_out_weight: bfloat16 [2048, 2048], P('tp', 'sp'), may hold values from -0.125 to 0.125
Outputs:
- mixed: bfloat16 [16384, 2048], P('sp', 'tp')
All inputs are finite; a program needn't handle non-finite values.
Results may differ from a plain program's by a relative error of at most 0.03.
Values may be sent and summed in bfloat16 or wider, within the bound.
No kernel may reach another device: no remote copies, remote signals or barrier semaphores. Data moves between devices by JAX's collectives and lax.ppermute only.
A program may use at most 128 MiB of HBM per device.

v0:
```python
import jax
import jax.numpy as jnp
from jax import lax
from jax.sharding import Mesh
from jax.sharding import PartitionSpec as P

BLOCK = 64
SP = ("sp_0", "sp_1", "sp_2")
EPS = 1e-06
LOWEST_LEVEL = -1e30


def in_order(blocks, dim):
    blocks = jnp.moveaxis(blocks, 0, dim)
    lengths = blocks.shape
    return blocks.reshape(*lengths[:dim], lengths[dim] * lengths[dim + 1], *lengths[dim + 2 :])


def copy_for_each(shard, axis):
    copies = jnp.broadcast_to(shard, (lax.axis_size(axis), *shard.shape))
    return lax.all_to_all(copies, axis, split_axis=0, concat_axis=0, tiled=True)


def gather_directly(shard, axis, dim):
    return in_order(copy_for_each(shard, axis), dim)


def sent_together(arrays, axis, dim, along):
    ends, at = ([], 0)
    for a in arrays[:-1]:
        at += a.shape[along]
        ends.append(at)
    both = jnp.concatenate(arrays, axis=along)
    return tuple(jnp.split(lax.all_gather(both, axis, axis=dim, tiled=True), ends, axis=along))


def shifted_2(value, axis, steps):
    count = lax.axis_size(axis)
    leading, last = (max(0, -steps), min(count, count - steps))
    return lax.ppermute(value, axis, [(source, source + steps) for source in range(leading, last)])


def neutral_like(shard, identity):
    return jax.tree.map(
        lambda a, e: jnp.broadcast_to(jnp.asarray(e, a.dtype), a.shape), shard, identity
    )


def entering(shard, axes, combine, identity):
    before = start = neutral_like(shard, identity)
    total = shard
    for axis in reversed(axes):
        devices, position = (lax.axis_size(axis), lax.axis_index(axis))
        pieces = jax.tree.map(
            lambda part, kind: lax.all_gather(part.astype(kind), axis),
            total,
            (jnp.bfloat16, jnp.bfloat16, jnp.bfloat16, jnp.bfloat16),
        )
        inside, total = (start, start)
        for k in range(devices):
            passed = k < position
            total = combine(
                total, jax.tree.map(lambda part, own: part[k].astype(own.dtype), pieces, shard)
            )
            inside = jax.tree.map(lambda new, old: jnp.where(passed, new, old), total, inside)
        before = combine(inside, before)
    return before


def of_everyone(shard, axis):
    return copy_for_each(shard, axis).sum(axis=0)


def turned_gather(arrays, axis, dims):
    turned = [jnp.moveaxis(a, dim, 0) for a, dim in zip(arrays, dims)]
    both = jnp.concatenate([t.reshape(len(t), -1) for t in turned], axis=1)
    out, at, finished = (lax.all_gather(both, axis, axis=0, tiled=True), 0, [])
    for t, dim in zip(turned, dims):
        share = out[:, at : at + t[0].size].reshape(-1, *t.shape[1:])
        finished.append(jnp.moveaxis(share, 0, dim))
        at += t[0].size
    return tuple(finished)


def cut_along(shard, dim, devices):
    before, after = (shard.shape[:dim], shard.shape[dim + 1 :])
    return jnp.moveaxis(shard.reshape(*before, devices, -1, *after), dim, 0)


def sum_at_owner(shard, axis, dim):
    blocks = cut_along(shard, dim, lax.axis_size(axis))
    arrived = lax.all_to_all(blocks, axis, split_axis=0, concat_axis=0, tiled=True)
    return arrived.astype(jnp.float32).sum(axis=0)


def block_step(carry, inputs):
    state, normal, level = carry
    query, key, value, gate_in, forget_log = inputs
    length = gate_in.shape[-1]
    scale = query.shape[-1] ** (-0.5)
    causal = jnp.tril(jnp.ones((length, length), dtype=bool))
    within = jnp.cumsum(forget_log, axis=-1)
    log_weight = within[:, :, None] - within[:, None, :] + gate_in[:, None, :]
    log_weight = jnp.where(causal, log_weight, -jnp.inf)
    carried = within + level[:, None]
    top = jnp.maximum(carried, jnp.max(log_weight, axis=-1))
    weight = jnp.exp(log_weight - top[:, :, None])
    carried_weight = jnp.exp(carried - top) * scale
    scores = jnp.einsum("htd,hsd->hts", query, key, preferred_element_type=jnp.float32) * (
        scale * weight
    )
    numer = jnp.einsum(
        "hts,hse->hte", scores.astype(jnp.bfloat16), value, preferred_element_type=jnp.float32
    )
    numer = numer + carried_weight[:, :, None] * jnp.einsum(
        "hed,htd->hte", state.astype(jnp.bfloat16), query, preferred_element_type=jnp.float32
    )
    denom = jnp.sum(scores, axis=-1) + carried_weight * jnp.einsum(
        "hd,htd->ht", normal.astype(jnp.bfloat16), query, preferred_element_type=jnp.float32
    )
    result = numer / jnp.maximum(jnp.abs(denom), 1.0)[:, :, None]
    last = within[:, -1]
    end_log = last[:, None] - within + gate_in
    new_level = jnp.maximum(last + level, jnp.max(end_log, axis=-1))
    keep = jnp.exp(last + level - new_level)
    fresh = jnp.exp(end_log - new_level[:, None])
    scaled_key = (fresh[:, :, None] * key).astype(jnp.bfloat16)
    new_state = keep[:, None, None] * state + jnp.einsum(
        "hse,hsd->hed", value, scaled_key, preferred_element_type=jnp.float32
    )
    new_normal = keep[:, None] * normal + jnp.sum(scaled_key.astype(jnp.float32), axis=1)
    return ((new_state, new_normal, new_level), result)


def depthwise(extended, kernel):
    taps = kernel.shape[0]
    length = extended.shape[0] - taps + 1
    total = extended[0:length] * kernel[0]
    for index in range(1, taps):
        total = total + extended[index : index + length] * kernel[index]
    return total


def merge_states(first, second):
    first_state, first_normal, first_level, first_total = first
    second_state, second_normal, second_level, second_total = second
    shifted = first_level + second_total
    level = jnp.maximum(shifted, second_level)
    older = jnp.exp(shifted - level)
    newer = jnp.exp(second_level - level)
    state = older[:, None, None] * first_state + newer[:, None, None] * second_state
    normal = older[:, None] * first_normal + newer[:, None] * second_normal
    return (state, normal, level, first_total + second_total)


def on_device(
    tokens,
    conv_value_weight,
    conv_gate_weight,
    conv_kernel,
    conv_norm_gain,
    query_weight,
    key_weight,
    value_weight,
    input_gate_weight,
    forget_gate_weight,
    input_offset,
    forget_offset,
    memory_norm_gain,
    conv_out_weight,
    memory_out_weight,
):
    length = tokens.shape[0]
    heads_here = input_gate_weight.shape[1]
    whole = gather_directly(tokens, "tp", 1)
    gathered = sent_together(
        (conv_value_weight, conv_gate_weight, query_weight, key_weight, value_weight), SP, 0, 1
    )
    folded = tuple(
        (jnp.dot(whole, weight, preferred_element_type=jnp.float32) for weight in gathered)
    )
    conv_value, conv_gate, query_flat, key_flat, value_flat = folded
    gate_pre = jnp.dot(whole, input_gate_weight, preferred_element_type=jnp.float32)
    forget_pre = jnp.dot(whole, forget_gate_weight, preferred_element_type=jnp.float32)
    glu = (conv_value * jax.nn.sigmoid(conv_gate)).astype(jnp.bfloat16)
    taps = conv_kernel.shape[0]
    head_dim = query_flat.shape[1] // heads_here

    def to_heads(flat):
        return flat.astype(jnp.bfloat16).reshape(length, heads_here, head_dim).transpose(1, 0, 2)

    query = to_heads(query_flat)
    key = to_heads(key_flat)
    value = to_heads(value_flat)
    gate_in = (gate_pre + input_offset).T
    forget_log = jax.nn.log_sigmoid(forget_pre + forget_offset).T
    within = jnp.cumsum(forget_log, axis=1)
    total = within[:, -1]
    end_log = total[:, None] - within + gate_in
    local_level = jnp.max(end_log, axis=1)
    fresh = jnp.exp(end_log - local_level[:, None])
    scaled_key = (fresh[:, :, None] * key).astype(jnp.bfloat16)
    local_state = jnp.einsum("hse,hsd->hed", value, scaled_key, preferred_element_type=jnp.float32)
    local_normal = jnp.sum(scaled_key.astype(jnp.float32), axis=1)
    blank_state = (
        jnp.zeros_like(local_state),
        jnp.zeros_like(local_normal),
        jnp.full_like(local_level, LOWEST_LEVEL),
        jnp.zeros_like(total),
    )
    prior = shifted_2(glu[length - (taps - 1) :], SP, 1)
    incoming = entering(
        (local_state, local_normal, local_level, total), SP, merge_states, blank_state
    )
    extended = jnp.concatenate([prior, glu], axis=0).astype(jnp.float32)
    conv = depthwise(extended, conv_kernel.astype(jnp.float32))
    blocks = length // BLOCK

    def split(array):
        return jnp.moveaxis(array.reshape((heads_here, blocks, BLOCK) + array.shape[2:]), 1, 0)

    _, hidden = lax.scan(
        block_step,
        tuple(incoming[:3]),
        (split(query), split(key), split(value), split(gate_in), split(forget_log)),
    )
    hidden = jnp.moveaxis(hidden, 0, 1).reshape(heads_here, length, head_dim)
    hidden_squares = jnp.sum(hidden * hidden, axis=(0, 2))
    channel_sum, channel_squares, memory_squares = (
        of_everyone(jnp.sum(conv, axis=1), "tp"),
        of_everyone(jnp.sum(conv * conv, axis=1), "tp"),
        of_everyone(hidden_squares, "tp"),
    )
    channels = conv.shape[1] * lax.axis_size("tp")
    mean = (channel_sum / channels)[:, None]
    variance = (channel_squares / channels)[:, None] - mean * mean
    conv_branch = jax.nn.silu((conv - mean) * lax.rsqrt(variance + EPS) * conv_norm_gain).astype(
        jnp.bfloat16
    )
    entries = heads_here * head_dim * lax.axis_size("tp")
    memory_scale = lax.rsqrt(memory_squares / entries + EPS)
    hidden = hidden * memory_scale[None, :, None]
    hidden = hidden * memory_norm_gain.reshape(heads_here, 1, head_dim)
    memory_branch = (
        hidden.transpose(1, 0, 2).reshape(length, heads_here * head_dim).astype(jnp.bfloat16)
    )
    conv_columns, memory_columns = turned_gather((conv_out_weight, memory_out_weight), SP, (1, 1))
    contract = (((0,), (1,)), ((), ()))
    summed = sum_at_owner(
        (
            lax.dot_general(conv_columns, conv_branch, contract, preferred_element_type=jnp.float32)
            + lax.dot_general(
                memory_columns, memory_branch, contract, preferred_element_type=jnp.float32
            )
        ).astype(jnp.bfloat16),
        "tp",
        0,
    )
    return summed.T.astype(jnp.bfloat16)


def solution(mesh):
    split = Mesh(mesh.devices.reshape(16, 4, 2, mesh.shape["tp"]), ("sp_0", "sp_1", "sp_2", "tp"))
    in_specs = (
        P(SP, "tp"),
        P(SP, "tp"),
        P(SP, "tp"),
        P(None, "tp"),
        P("tp"),
        P(SP, "tp"),
        P(SP, "tp"),
        P(SP, "tp"),
        P(None, "tp"),
        P(None, "tp"),
        P(SP, "tp"),
        P(SP, "tp"),
        P("tp"),
        P("tp", SP),
        P("tp", SP),
    )
    out_specs = P(SP, "tp")
    return jax.shard_map(
        on_device, mesh=split, in_specs=in_specs, out_specs=out_specs, check_vma=False
    )
```

profile of v0, /device:TPU:1, one launch (start us, length us, event | category | flops | bytes accessed | tf_op | source)
XLA Modules:
  0.0 445.2 jit_solution(18037875826479777491)
XLA Ops:
  6.5 0.7 constant_dynamic-update-slice_fusion.4
  7.2 0.7 constant_dynamic-update-slice_fusion.3
  7.9 0.7 constant_dynamic-update-slice_fusion.2
  8.7 0.7 constant_dynamic-update-slice_fusion.1
  9.4 0.7 constant_dynamic-update-slice_fusion
  10.1 0.6 copy-done.2
  10.8 1.0 copy.62
  11.8 0.9 broadcast_in_dim.26
  12.7 5.0 %all-to-all-start = ((bf16[4,128,512]{1,2,0:T(8,128)(2,1)}), bf16[4,128,512]{1,2,0:T(8,128)(2,1)S(1)}, u32[]{:S(2)}, u32[]{:S(2)}) async-start(bf16[4,128,512]{1,2,0:T(8,128)(2,1)} %broadcast_in_dim.26), calls=%async_computation | async-start | bytes 1048576 | tf_op jit(solution)/shard_map/all_to_all | solution.py:21
  17.7 1.3 dynamic-slice
  19.6 5.0 %all-to-all-done = bf16[4,128,512]{1,2,0:T(8,128)(2,1)S(1)} async-done(((bf16[4,128,512]{1,2,0:T(8,128)(2,1)}), bf16[4,128,512]{1,2,0:T(8,128)(2,1)S(1)}, u32[]{:S(2)}, u32[]{:S(2)}) %all-to-all-start) | async-done | bytes 524320 | tf_op jit(solution)/shard_map/all_to_all | solution.py:21
  24.6 0.9 fusion.219
  26.0 1.0 fusion.329
  27.7 8.5 %all-reduce.2 = (bf16[4]{0:T(256)(128)(2,1)S(1)}, bf16[4]{0:T(256)(128)(2,1)S(1)}) all-reduce(bf16[4]{0:T(256)(128)(2,1)S(1)} %dynamic-update-slice.1, bf16[4]{0:T(256)(128)(2,1)S(1)} %dynamic-update-slice), channel_id=3, replica_groups=mesh['sp_0'=16,'sp_1'=4,'sp_2'=2,'tp'=4] {'sp_2'}, use_global_device_ids=true, to_apply=%add.1 | all-reduce | flops 8 | bytes 32
  36.3 5.6 %all-gather.4 = bf16[4,1,2]{2,1,0:T(2,128)(2,1)S(1)} all-gather(bf16[1,1,2]{2,1,0:T(2,128)(2,1)S(1)} %get-tuple-element.249), channel_id=1, replica_groups=mesh['sp_0'=16,'sp_1'=4,'sp_2'=2,'tp'=4] {'sp_1'}, dimensions={0}, use_global_device_ids=true | all-gather | bytes 20 | tf_op jit(solution)/shard_map/all_gather | solution.py:55
  41.9 7.2 %all-gather.6 = bf16[4,1,2]{2,1,0:T(2,128)(2,1)S(1)} all-gather(bf16[1,1,2]{2,1,0:T(2,128)(2,1)S(1)} %get-tuple-element.250), channel_id=1, replica_groups=mesh['sp_0'=16,'sp_1'=4,'sp_2'=2,'tp'=4] {'sp_1'}, dimensions={0}, use_global_device_ids=true | all-gather | bytes 20 | tf_op jit(solution)/shard_map/all_gather | solution.py:55
  49.1 26.7 %all-gather.7 = bf16[16,1,2]{2,1,0:T(2,128)(2,1)S(1)} all-gather(bf16[1,1,2]{2,1,0:T(2,128)(2,1)S(1)} %get-tuple-element.238), channel_id=1, replica_groups=mesh['sp_0'=16,'sp_1'=4,'sp_2'=2,'tp'=4] {'sp_0'}, dimensions={0}, use_global_device_ids=true | all-gather | bytes 68 | tf_op jit(solution)/shard_map/all_gather | solution.py:55
  75.8 20.2 %all-gather.5 = bf16[16,1,2]{2,1,0:T(2,128)(2,1)S(1)} all-gather(bf16[1,1,2]{2,1,0:T(2,128)(2,1)S(1)} %get-tuple-element.239), channel_id=1, replica_groups=mesh['sp_0'=16,'sp_1'=4,'sp_2'=2,'tp'=4] {'sp_0'}, dimensions={0}, use_global_device_ids=true | all-gather | bytes 68 | tf_op jit(solution)/shard_map/all_gather | solution.py:55
  96.3 67.5 %all-gather.16.cloned.1.call-done = bf16[2048,2048]{1,0:T(8,128)(2,1)} async-done(((bf16[16,2048]{1,0:T(8,128)(2,1)}), bf16[2048,2048]{1,0:T(8,128)(2,1)}) %all-gather.16.cloned.1.call-update) | async-done | bytes 8388624 | tf_op jit(solution)/shard_map/all_gather | solution.py:34
  163.8 2.3 fusion.40
  166.4 2.4 fusion.37
  169.0 2.2 all-gather.2
  171.2 0.9 fusion.88
  172.2 24.1 %all-gather.18.cloned.1.call-done = bf16[4,2,256,256]{3,2,1,0:T(8,128)(2,1)} async-done(((bf16[1,2,256,256]{3,2,1,0:T(8,128)(2,1)}), bf16[4,2,256,256]{3,2,1,0:T(8,128)(2,1)}) %all-gather.18.cloned.1.call-update) | async-done | bytes 1048592 | tf_op jit(solution)/shard_map/all_gather | solution.py:55
  196.3 2.2 fusion.66
  198.6 0.6 pad_maximum_fusion
  199.8 4.2 all-gather.8
  204.1 6.5 %all_gather.72 = bf16[4,2,256]{2,1,0:T(2,128)(2,1)S(1)} all-gather(bf16[1,2,256]{2,1,0:T(2,128)(2,1)S(1)} %fusion.217), channel_id=1, replica_groups=mesh['sp_0'=16,'sp_1'=4,'sp_2'=2,'tp'=4] {'sp_1'}, dimensions={0}, use_global_device_ids=true | all-gather | bytes 5120 | tf_op jit(solution)/shard_map/all_gather | solution.py:55
  210.5 1.6 fusion.55
  212.1 1.6 fusion.51
  213.7 4.5 %collective-permute-start = (bf16[30,256]{1,0:T(8,128)(2,1)S(1)}, bf16[30,256]{1,0:T(8,128)(2,1)S(1)}, u32[]{:S(2)}, u32[]{:S(2)}) collective-permute-start(bf16[30,256]{1,0:T(8,128)(2,1)S(1)} %slice.672), channel_id=1, source_target_pairs={{0,4},{4,8},{8,12},{12,16},{16,20},{20,24},{24,28},{28,32},{32,36}... | collective-permute-start | bytes 46088 | tf_op jit(solution)/shard_map/ppermute | solution.py:40
  218.2 2.4 fusion.43
  221.3 0.6 broadcast_in_dim.28
  221.9 4.0 all-to-all-start.2
  225.9 25.9 %all_gather.73 = bf16[16,2,256]{2,1,0:T(2,128)(2,1)S(1)} all-gather(bf16[1,2,256]{2,1,0:T(2,128)(2,1)S(1)} %fusion.182), channel_id=1, replica_groups=mesh['sp_0'=16,'sp_1'=4,'sp_2'=2,'tp'=4] {'sp_0'}, dimensions={0}, use_global_device_ids=true | all-gather | bytes 17408 | tf_op jit(solution)/shard_map/all_gather | solution.py:55
  251.8 0.6 broadcast_in_dim.27
  252.3 4.6 %all-to-all-start.1 = ((f32[4,1,128]{2,1,0:T(1,128)}), f32[4,1,128]{2,1,0:T(1,128)S(1)}, u32[]{:S(2)}, u32[]{:S(2)}) async-start(f32[4,1,128]{2,1,0:T(1,128)} %broadcast_in_dim.27), calls=%async_computation.1 | async-start | bytes 4096 | tf_op jit(solution)/shard_map/all_to_all | solution.py:21
  257.3 3.9 all-to-all-done.1
  261.2 9.4 %all-gather.20.cloned.1.call-done = bf16[16,2,256,256]{3,2,1,0:T(8,128)(2,1)} async-done(((bf16[1,2,256,256]{3,2,1,0:T(8,128)(2,1)}), bf16[16,2,256,256]{3,2,1,0:T(8,128)(2,1)}) %all-gather.20.cloned.1.call-update) | async-done | bytes 4194320 | tf_op jit(solution)/shard_map/all_gather | solution.py:55
  270.6 4.5 %fusion.78 = f32[2,256,256]{2,1,0:T(8,128)S(1)} fusion(bf16[16,2,256,256]{3,2,1,0:T(8,128)(2,1)} %all-gather.20.cloned.1.call-done, f32[2]{0:T(128)S(1)} %get-tuple-element.247, f32[2]{0:T(128)S(1)} %get-tuple-element.241, f32[2]{0:T(128)S(1)} %get-tuple-element.246, f32[2]{0:T(128)S(1)} %get-tuple-element.245, f32[2]{0:T(128)S(1)} %get-tuple-element.240, ...), kind=kLoop, calls=%fused_computation.107 | loop fusion | flops 15073280 | bytes 6291878 | tf_op jit(solution)/shard_map/add | solution.py:151
  275.1 4.7 %while.16 = (s32[]{:T(128)}, f32[2,256,256]{2,1,0:T(8,128)S(1)}, f32[2,256]{1,0:T(2,128)S(1)}, f32[2]{0:T(128)S(1)}, f32[2,2,64,256]{3,2,0,1:T(8,128)S(1)}, /*in...) while((s32[]{:T(128)}, f32[2,256,256]{2,1,0:T(8,128)S(1)}, ...), condition=%wide.region_13.14_spmd, body=%wide.region_7.13_spmd.sunk | while | flops 42875268 | bytes 2589965 | solution.py:222
  280.0 0.6 broadcast_in_dim.33
  280.6 4.0 all-to-all-start.3
  284.6 136.1 %all-gather.14.cloned.1.call-done = bf16[2048,768]{1,0:T(8,128)(2,1)} async-done(((bf16[16,768]{1,0:T(8,128)(2,1)}), bf16[2048,768]{1,0:T(8,128)(2,1)}) %all-gather.14.cloned.1.call-update) | async-done | bytes 3145744 | tf_op jit(solution)/shard_map/all_gather | solution.py:77
  420.7 1.7 fusion.57
  422.7 2.3 fusion.29
  425.0 12.8 %all_to_all.28 = bf16[4,512,128]{2,1,0:T(8,128)(2,1)S(1)} all-to-all(bf16[4,512,128]{2,1,0:T(8,128)(2,1)S(1)} %bitcast.981), channel_id=1, replica_groups=mesh['sp_0'=16,'sp_1'=4,'sp_2'=2,'tp'=4] {'tp'}, dimensions={0} | all-to-all | bytes 1048576 | tf_op jit(solution)/shard_map/all_to_all | solution.py:92
  437.9 0.8 copy.77
  (111 shorter events, 8.9 us)
Async XLA Ops:
  6.5 19.5 %copy-start = (bf16[2048,2]{0,1:T(2,128)(2,1)S(1)}, bf16[2048,2]{0,1:T(2,128)(2,1)}, u32[]{:S(2)}) copy-start(bf16[2048,2]{0,1:T(2,128)(2,1)} %param.25) | copy-start | bytes 24580
  6.5 157.3 %all-gather.16.cloned.1.call-start = ((), (), s32[]{:S(2)}) async-start(), calls=%async_computation.6 | async-start | bytes 8454144 | tf_op jit(solution)/shard_map/all_gather | solution.py:34
  10.1 0.6 copy-start.2
  12.7 11.9 %all-to-all-start = ((bf16[4,128,512]{1,2,0:T(8,128)(2,1)}), bf16[4,128,512]{1,2,0:T(8,128)(2,1)S(1)}, u32[]{:S(2)}, u32[]{:S(2)}) async-start(bf16[4,128,512]{1,2,0:T(8,128)(2,1)} %broadcast_in_dim.26), calls=%async_computation | async-start | bytes 1048576 | tf_op jit(solution)/shard_map/all_to_all | solution.py:21
  17.7 178.6 %all-gather.18.cloned.1.call-start = ((), (), s32[]{:S(2)}) async-start(), calls=%async_computation.7 | async-start | bytes 1310720 | tf_op jit(solution)/shard_map/all_gather | solution.py:55
  166.3 32.3 %copy-start.4 = (bf16[512,16]{0,1:T(8,128)(2,1)S(1)}, bf16[512,16]{0,1:T(8,128)(2,1)}, u32[]{:S(2)}) copy-start(bf16[512,16]{0,1:T(8,128)(2,1)} %param.31) | copy-start | bytes 49156
  166.3 32.3 %copy-start.5 = (bf16[256,16]{0,1:T(8,128)(2,1)S(1)}, bf16[256,16]{0,1:T(8,128)(2,1)}, u32[]{:S(2)}) copy-start(bf16[256,16]{0,1:T(8,128)(2,1)} %param.30) | copy-start | bytes 24580
  166.3 32.9 %copy-start.3 = (bf16[31,256]{1,0:T(8,128)(2,1)S(1)}, bf16[31,256]{1,0:T(8,128)(2,1)}, u32[]{:S(2)}) copy-start(bf16[31,256]{1,0:T(8,128)(2,1)} %param.20) | copy-start | bytes 47620
  166.3 33.0 %copy-start.6 = (f32[512]{0:T(512)S(1)}, f32[512]{0:T(512)}, u32[]{:S(2)}) copy-start(f32[512]{0:T(512)} %param.29) | copy-start | bytes 6148
  172.1 98.4 %all-gather.20.cloned.1.call-start = ((), (), s32[]{:S(2)}) async-start(), calls=%async_computation.8 | async-start | bytes 4456448 | tf_op jit(solution)/shard_map/all_gather | solution.py:55
  198.6 222.1 %all-gather.14.cloned.1.call-start = ((), (), s32[]{:S(2)}) async-start(), calls=%async_computation.5 | async-start | bytes 3170304 | tf_op jit(solution)/shard_map/all_gather | solution.py:77
  213.7 56.9 %copy-start.1 = (bf16[4,2,256,256]{3,2,1,0:T(8,128)(2,1)S(1)}, bf16[4,2,256,256]{3,2,1,0:T(8,128)(2,1)}, u32[]{:S(2)}) copy-start(bf16[4,2,256,256]{3,2,1,0:T(8,128)(2,1)} %all-gather.18.cloned.1.call-done) | copy-start | bytes 3145732
  213.7 7.0 %collective-permute-start = (bf16[30,256]{1,0:T(8,128)(2,1)S(1)}, bf16[30,256]{1,0:T(8,128)(2,1)S(1)}, u32[]{:S(2)}, u32[]{:S(2)}) collective-permute-start(bf16[30,256]{1,0:T(8,128)(2,1)S(1)} %slice.672), channel_id=1, source_target_pairs={{0,4},{4,8},{8,12},{12,16},{16,20},{20,24},{24,28},{28,32},{32,36}... | collective-permute-start | bytes 46088 | tf_op jit(solution)/shard_map/ppermute | solution.py:40
  221.9 29.9 %all-to-all-start.2 = ((f32[4,1,128]{2,1,0:T(1,128)}), f32[4,1,128]{2,1,0:T(1,128)S(1)}, u32[]{:S(2)}, u32[]{:S(2)}) async-start(f32[4,1,128]{2,1,0:T(1,128)} %broadcast_in_dim.28), calls=%async_computation.2 | async-start | bytes 4096 | tf_op jit(solution)/shard_map/all_to_all | solution.py:21
  252.3 8.9 %all-to-all-start.1 = ((f32[4,1,128]{2,1,0:T(1,128)}), f32[4,1,128]{2,1,0:T(1,128)S(1)}, u32[]{:S(2)}, u32[]{:S(2)}) async-start(f32[4,1,128]{2,1,0:T(1,128)} %broadcast_in_dim.27), calls=%async_computation.1 | async-start | bytes 4096 | tf_op jit(solution)/shard_map/all_to_all | solution.py:21
  275.1 145.6 %copy-start.7 = (f32[256]{0:T(256)S(1)}, f32[256]{0:T(256)}, u32[]{:S(2)}) copy-start(f32[256]{0:T(256)} %param.21) | copy-start | bytes 3076
  280.6 141.8 %all-to-all-start.3 = ((f32[4,1,128]{2,1,0:T(1,128)}), f32[4,1,128]{2,1,0:T(1,128)S(1)}, u32[]{:S(2)}, u32[]{:S(2)}) async-start(f32[4,1,128]{2,1,0:T(1,128)} %broadcast_in_dim.33), calls=%async_computation.3 | async-start | bytes 4096 | tf_op jit(solution)/shard_map/all_to_all | solution.py:21
Sparse Core Ops, SparseCore 0:
  10.9 152.9 all-gather.15
  172.3 24.0 all-gather.17
  198.7 71.8 all-gather.19
  273.6 147.0 all-gather.13
where the time goes:
time: 446 us; the launch traced here: 445 us
  waiting for transfers between devices  246 us (55%)
  blocking collectives  120 us (27%)
  starting transfers between devices  22.2 us (5%)
  matrix products  18.6 us (4%)
  between operations  14.1 us (3%)
  other arithmetic  12.5 us (3%)
  local copies, waits for them, and re-layouts  12 us (3%)
    all_gather x1, waiting for transfers between devices, turned_gather(): out, at, finished = (lax.all_gather(both, axis, axis=0, tiled=True), 0, [])  136 us
    all_gather x8, blocking collectives, entering(): lax.all_gather(part.astype(kind), axis)  98.4 us
    all_gather x1, waiting for transfers between devices, sent_together(): lax.all_gather(both, axis, axis=dim, tiled=True)  67.5 us
    all_gather x2, waiting for transfers between devices, entering(): lax.all_gather(part.astype(kind), axis)  33.5 us
    all_to_all x4, starting transfers between devices, copy_for_each(): return lax.all_to_all(copies, axis, split_axis=0, concat_axis=0, tiled=True)  17.6 us
    all_to_all x1, blocking collectives, sum_at_owner(): lax.all_to_all(blocks, axis, split_axis=0, concat_axis=0, tiled=True)  12.8 us
    dot_general x5, matrix products, on_device(): jnp.dot(whole, weight, preferred_element_type=jnp.float32)  10.2 us
  transfers between devices with their start and end apart: 9, of which 6 were waited for; matrix products, arithmetic and copies ran while one was open for 6% of the time, Pallas kernels for 0%

commit v1 on v0

--- a/solution.py
+++ b/solution.py
@@ -74,7 +74,13 @@
 def turned_gather(arrays, axis, dims):
     turned = [jnp.moveaxis(a, dim, 0) for a, dim in zip(arrays, dims)]
     both = jnp.concatenate([t.reshape(len(t), -1) for t in turned], axis=1)
-    out, at, finished = (lax.all_gather(both, axis, axis=0, tiled=True), 0, [])
+    out, at, finished = (
+        jnp.concatenate(
+            lax.all_to_all(jnp.stack([both] * lax.axis_size(axis)), axis, 0, 0), axis=0
+        ),
+        0,
+        [],
+    )
     for t, dim in zip(turned, dims):
         share = out[:, at : at + t[0].size].reshape(-1, *t.shape[1:])
         finished.append(jnp.moveaxis(share, 0, dim))

time: 446 us -> 467 us (1.047); the launches traced: 445 us -> 458 us
  waiting for transfers between devices: 246 us -> 104 us
  blocking collectives: 120 us -> 256 us
  starting transfers between devices: 22.2 us -> 39.4 us
    all_gather x1 -> x0, waiting for transfers between devices: 136 us -> none  [turned_gather(): out, at, finished = (lax.all_gather(both, axis, axis=0, tiled=True), 0, [])]
    all_gather x8, blocking collectives: 98.4 us -> 231 us  [entering(): lax.all_gather(part.astype(kind), axis)]
    all_to_all x0 -> x1, starting transfers between devices: none -> 22.2 us  [turned_gather(): lax.all_to_all(jnp.stack([both] * lax.axis_size(axis)), axis, 0, 0)]
    all_gather x2, waiting for transfers between devices: 33.5 us -> 24.1 us  [entering(): lax.all_gather(part.astype(kind), axis)]
    all_to_all x0 -> x1, blocking collectives: none -> 7.94 us  [copy_for_each(): return lax.all_to_all(copies, axis, split_axis=0, concat_axis=0, tiled=True)]
    all_to_all x4 -> x3, starting transfers between devices: 17.6 us -> 12.5 us  [copy_for_each(): return lax.all_to_all(copies, axis, split_axis=0, concat_axis=0, tiled=True)]
    all_to_all x4 -> x3, waiting for transfers between devices: 8.85 us -> 11.4 us  [copy_for_each(): return lax.all_to_all(copies, axis, split_axis=0, concat_axis=0, tiled=True)]
  transfers between devices with their start and end apart: 9 -> 8, of which waited for: 6 -> 6; matrix products, arithmetic and copies ran while one was open for 6% -> 6% of each run, Pallas kernels for 0% -> 0%
where the time goes in v1:
time: 467 us; the launch traced here: 458 us
  blocking collectives  256 us (55%)
  waiting for transfers between devices  104 us (22%)
  starting transfers between devices  39.4 us (8%)
  matrix products  18.8 us (4%)
  between operations  14.1 us (3%)
  local copies, waits for them, and re-layouts  13.3 us (3%)
  other arithmetic  12 us (3%)
    all_gather x8, blocking collectives, entering(): lax.all_gather(part.astype(kind), axis)  231 us
    all_gather x1, waiting for transfers between devices, sent_together(): lax.all_gather(both, axis, axis=dim, tiled=True)  67.5 us
    all_gather x2, waiting for transfers between devices, entering(): lax.all_gather(part.astype(kind), axis)  24.1 us
    all_to_all x1, starting transfers between devices, turned_gather(): lax.all_to_all(jnp.stack([both] * lax.axis_size(axis)), axis, 0, 0)  22.2 us
    all_to_all x3, starting transfers between devices, copy_for_each(): return lax.all_to_all(copies, axis, split_axis=0, concat_axis=0, tiled=True)  12.5 us
    all_to_all x3, waiting for transfers between devices, copy_for_each(): return lax.all_to_all(copies, axis, split_axis=0, concat_axis=0, tiled=True)  11.4 us
    dot_general x5, matrix products, on_device(): jnp.dot(whole, weight, preferred_element_type=jnp.float32)  10.4 us
  transfers between devices with their start and end apart: 8, of which 6 were waited for; matrix products, arithmetic and copies ran while one was open for 6% of the time, Pallas kernels for 0%

profile of v1, /device:TPU:1, one launch (start us, length us, event | category | flops | bytes accessed | tf_op | source)
XLA Modules:
  0.0 458.0 jit_solution(9289053608185997120)
XLA Ops:
  6.5 0.7 constant_dynamic-update-slice_fusion.4
  7.2 0.7 constant_dynamic-update-slice_fusion.3
  7.9 0.7 constant_dynamic-update-slice_fusion.2
  8.7 0.7 constant_dynamic-update-slice_fusion.1
  9.4 0.7 constant_dynamic-update-slice_fusion
  10.1 0.6 copy-done.2
  10.8 1.0 copy.62
  11.8 0.9 broadcast_in_dim.26
  12.7 5.0 %all-to-all-start.1 = ((bf16[4,128,512]{1,2,0:T(8,128)(2,1)}), bf16[4,128,512]{1,2,0:T(8,128)(2,1)S(1)}, u32[]{:S(2)}, u32[]{:S(2)}) async-start(bf16[4,128,512]{1,2,0:T(8,128)(2,1)} %broadcast_in_dim.26), calls=%async_computation.1 | async-start | bytes 1048576 | tf_op jit(solution)/shard_map/all_to_all | solution.py:21
  17.7 1.3 dynamic-slice
  19.6 5.0 %all-to-all-done.1 = bf16[4,128,512]{1,2,0:T(8,128)(2,1)S(1)} async-done(((bf16[4,128,512]{1,2,0:T(8,128)(2,1)}), bf16[4,128,512]{1,2,0:T(8,128)(2,1)S(1)}, u32[]{:S(2)}, u32[]{:S(2)}) %all-to-all-start.1) | async-done | bytes 524320 | tf_op jit(solution)/shard_map/all_to_all | solution.py:21
  24.6 0.9 fusion.219
  26.0 1.0 fusion.329
  27.7 8.5 %all-reduce.2 = (bf16[4]{0:T(256)(128)(2,1)S(1)}, bf16[4]{0:T(256)(128)(2,1)S(1)}) all-reduce(bf16[4]{0:T(256)(128)(2,1)S(1)} %dynamic-update-slice.1, bf16[4]{0:T(256)(128)(2,1)S(1)} %dynamic-update-slice), channel_id=3, replica_groups=mesh['sp_0'=16,'sp_1'=4,'sp_2'=2,'tp'=4] {'sp_2'}, use_global_device_ids=true, to_apply=%add.1 | all-reduce | flops 8 | bytes 32
  36.3 5.6 %all-gather.4 = bf16[4,1,2]{2,1,0:T(2,128)(2,1)S(1)} all-gather(bf16[1,1,2]{2,1,0:T(2,128)(2,1)S(1)} %get-tuple-element.249), channel_id=1, replica_groups=mesh['sp_0'=16,'sp_1'=4,'sp_2'=2,'tp'=4] {'sp_1'}, dimensions={0}, use_global_device_ids=true | all-gather | bytes 20 | tf_op jit(solution)/shard_map/all_gather | solution.py:55
  41.9 7.2 %all-gather.6 = bf16[4,1,2]{2,1,0:T(2,128)(2,1)S(1)} all-gather(bf16[1,1,2]{2,1,0:T(2,128)(2,1)S(1)} %get-tuple-element.250), channel_id=1, replica_groups=mesh['sp_0'=16,'sp_1'=4,'sp_2'=2,'tp'=4] {'sp_1'}, dimensions={0}, use_global_device_ids=true | all-gather | bytes 20 | tf_op jit(solution)/shard_map/all_gather | solution.py:55
  49.1 26.7 %all-gather.7 = bf16[16,1,2]{2,1,0:T(2,128)(2,1)S(1)} all-gather(bf16[1,1,2]{2,1,0:T(2,128)(2,1)S(1)} %get-tuple-element.238), channel_id=1, replica_groups=mesh['sp_0'=16,'sp_1'=4,'sp_2'=2,'tp'=4] {'sp_0'}, dimensions={0}, use_global_device_ids=true | all-gather | bytes 68 | tf_op jit(solution)/shard_map/all_gather | solution.py:55
  75.8 20.2 %all-gather.5 = bf16[16,1,2]{2,1,0:T(2,128)(2,1)S(1)} all-gather(bf16[1,1,2]{2,1,0:T(2,128)(2,1)S(1)} %get-tuple-element.239), channel_id=1, replica_groups=mesh['sp_0'=16,'sp_1'=4,'sp_2'=2,'tp'=4] {'sp_0'}, dimensions={0}, use_global_device_ids=true | all-gather | bytes 68 | tf_op jit(solution)/shard_map/all_gather | solution.py:55
  96.3 67.5 %all-gather.13.cloned.1.call-done = bf16[2048,2048]{1,0:T(8,128)(2,1)} async-done(((bf16[16,2048]{1,0:T(8,128)(2,1)}), bf16[2048,2048]{1,0:T(8,128)(2,1)}) %all-gather.13.cloned.1.call-update) | async-done | bytes 8388624 | tf_op jit(solution)/shard_map/all_gather | solution.py:34
  163.8 2.3 fusion.40
  166.3 2.4 fusion.37
  169.0 2.2 all-gather.2
  171.2 0.9 fusion.88
  172.2 24.1 %all-gather.15.cloned.1.call-done = bf16[4,2,256,256]{3,2,1,0:T(8,128)(2,1)} async-done(((bf16[1,2,256,256]{3,2,1,0:T(8,128)(2,1)}), bf16[4,2,256,256]{3,2,1,0:T(8,128)(2,1)}) %all-gather.15.cloned.1.call-update) | async-done | bytes 1048592 | tf_op jit(solution)/shard_map/all_gather | solution.py:55
  196.3 2.2 fusion.66
  198.6 1.6 fusion.55
  200.2 1.6 fusion.51
  201.8 4.6 %collective-permute-start = (bf16[30,256]{1,0:T(8,128)(2,1)S(1)}, bf16[30,256]{1,0:T(8,128)(2,1)S(1)}, u32[]{:S(2)}, u32[]{:S(2)}) collective-permute-start(bf16[30,256]{1,0:T(8,128)(2,1)S(1)} %slice.672), channel_id=1, source_target_pairs={{0,4},{4,8},{8,12},{12,16},{16,20},{20,24},{24,28},{28,32},{32,36}... | collective-permute-start | bytes 46088 | tf_op jit(solution)/shard_map/ppermute | solution.py:40
  206.5 0.8 collective-permute-done
  207.3 0.6 fusion.309
  207.9 7.9 %all_to_all.33 = f32[4,1,128]{2,1,0:T(1,128)S(1)} all-to-all(f32[4,1,128]{2,1,0:T(1,128)S(1)} %broadcast_in_dim.28), channel_id=1, replica_groups=mesh['sp_0'=16,'sp_1'=4,'sp_2'=2,'tp'=4] {'tp'}, dimensions={0} | all-to-all | bytes 4096 | tf_op jit(solution)/shard_map/all_to_all | solution.py:21
  216.4 3.2 all-to-all-start.2
  219.7 4.1 all-to-all-done.2
  223.8 1.9 stack.2
  225.6 22.2 %all-to-all-start = ((bf16[128,16,768]{2,1,0:T(8,128)(2,1)}), bf16[128,16,768]{2,1,0:T(8,128)(2,1)}, u32[]{:S(2)}, u32[]{:S(2)}) async-start(bf16[128,16,768]{2,1,0:T(8,128)(2,1)} %stack.2), calls=%async_computation | async-start | bytes 6291456 | tf_op jit(solution)/shard_map/all_to_all | solution.py:79
  248.3 2.5 fusion.43
  251.0 2.4 all-gather.8
  253.5 8.0 %all_gather.68 = bf16[4,2,256]{2,1,0:T(2,128)(2,1)S(1)} all-gather(bf16[1,2,256]{2,1,0:T(2,128)(2,1)S(1)} %fusion.217), channel_id=1, replica_groups=mesh['sp_0'=16,'sp_1'=4,'sp_2'=2,'tp'=4] {'sp_1'}, dimensions={0}, use_global_device_ids=true | all-gather | bytes 5120 | tf_op jit(solution)/shard_map/all_gather | solution.py:55
  261.6 158.3 %all_gather.69 = bf16[16,2,256]{2,1,0:T(2,128)(2,1)S(1)} all-gather(bf16[1,2,256]{2,1,0:T(2,128)(2,1)S(1)} %fusion.182), channel_id=1, replica_groups=mesh['sp_0'=16,'sp_1'=4,'sp_2'=2,'tp'=4] {'sp_0'}, dimensions={0}, use_global_device_ids=true | all-gather | bytes 17408 | tf_op jit(solution)/shard_map/all_gather | solution.py:55
  420.2 4.7 %fusion.78 = f32[2,256,256]{2,1,0:T(8,128)S(1)} fusion(bf16[16,2,256,256]{3,2,1,0:T(8,128)(2,1)} %all-gather.17.cloned.1.call-done, f32[2]{0:T(128)S(1)} %get-tuple-element.247, f32[2]{0:T(128)S(1)} %get-tuple-element.241, f32[2]{0:T(128)S(1)} %get-tuple-element.246, f32[2]{0:T(128)S(1)} %get-tuple-element.245, f32[2]{0:T(128)S(1)} %get-tuple-element.240, ...), kind=kLoop, calls=%fused_computation.107 | loop fusion | flops 15073280 | bytes 6291878 | tf_op jit(solution)/shard_map/add | solution.py:157
  424.9 4.7 %while.16 = (s32[]{:T(128)}, f32[2,256,256]{2,1,0:T(8,128)S(1)}, f32[2,256]{1,0:T(2,128)S(1)}, f32[2]{0:T(128)S(1)}, f32[2,2,64,256]{3,2,0,1:T(8,128)S(1)}, /*in...) while((s32[]{:T(128)}, f32[2,256,256]{2,1,0:T(8,128)S(1)}, ...), condition=%wide.region_13.14_spmd, body=%wide.region_7.13_spmd.sunk | while | flops 42875268 | bytes 2589965 | solution.py:228
  429.8 0.6 broadcast_in_dim.33
  430.4 4.3 all-to-all-start.4
  434.7 1.7 fusion.57
  436.4 2.3 all-to-all-done.4
  439.0 2.3 fusion.29
  441.3 9.3 %all_to_all.34 = bf16[4,512,128]{2,1,0:T(8,128)(2,1)S(1)} all-to-all(bf16[4,512,128]{2,1,0:T(8,128)(2,1)S(1)} %bitcast.982), channel_id=1, replica_groups=mesh['sp_0'=16,'sp_1'=4,'sp_2'=2,'tp'=4] {'tp'}, dimensions={0} | all-to-all | bytes 1048576 | tf_op jit(solution)/shard_map/all_to_all | solution.py:98
  450.7 0.8 copy.77
  (110 shorter events, 8.9 us)
Async XLA Ops:
  6.5 19.5 %copy-start = (bf16[2048,2]{0,1:T(2,128)(2,1)S(1)}, bf16[2048,2]{0,1:T(2,128)(2,1)}, u32[]{:S(2)}) copy-start(bf16[2048,2]{0,1:T(2,128)(2,1)} %param.25) | copy-start | bytes 24580
  6.5 157.3 %all-gather.13.cloned.1.call-start = ((), (), s32[]{:S(2)}) async-start(), calls=%async_computation.6 | async-start | bytes 8454144 | tf_op jit(solution)/shard_map/all_gather | solution.py:34
  10.1 0.6 copy-start.2
  12.7 11.9 %all-to-all-start.1 = ((bf16[4,128,512]{1,2,0:T(8,128)(2,1)}), bf16[4,128,512]{1,2,0:T(8,128)(2,1)S(1)}, u32[]{:S(2)}, u32[]{:S(2)}) async-start(bf16[4,128,512]{1,2,0:T(8,128)(2,1)} %broadcast_in_dim.26), calls=%async_computation.1 | async-start | bytes 1048576 | tf_op jit(solution)/shard_map/all_to_all | solution.py:21
  17.7 178.6 %all-gather.15.cloned.1.call-start = ((), (), s32[]{:S(2)}) async-start(), calls=%async_computation.7 | async-start | bytes 1310720 | tf_op jit(solution)/shard_map/all_gather | solution.py:55
  168.7 29.9 %copy-start.3 = (bf16[31,256]{1,0:T(8,128)(2,1)S(1)}, bf16[31,256]{1,0:T(8,128)(2,1)}, u32[]{:S(2)}) copy-start(bf16[31,256]{1,0:T(8,128)(2,1)} %param.20) | copy-start | bytes 47620
  172.1 248.1 %all-gather.17.cloned.1.call-start = ((), (), s32[]{:S(2)}) async-start(), calls=%async_computation.8 | async-start | bytes 4456448 | tf_op jit(solution)/shard_map/all_gather | solution.py:55
  200.2 19.5 %copy-start.4 = (bf16[512,16]{0,1:T(8,128)(2,1)S(1)}, bf16[512,16]{0,1:T(8,128)(2,1)}, u32[]{:S(2)}) copy-start(bf16[512,16]{0,1:T(8,128)(2,1)} %param.31) | copy-start | bytes 49156
  200.2 19.5 %copy-start.5 = (bf16[256,16]{0,1:T(8,128)(2,1)S(1)}, bf16[256,16]{0,1:T(8,128)(2,1)}, u32[]{:S(2)}) copy-start(bf16[256,16]{0,1:T(8,128)(2,1)} %param.30) | copy-start | bytes 24580
  201.8 5.4 %collective-permute-start = (bf16[30,256]{1,0:T(8,128)(2,1)S(1)}, bf16[30,256]{1,0:T(8,128)(2,1)S(1)}, u32[]{:S(2)}, u32[]{:S(2)}) collective-permute-start(bf16[30,256]{1,0:T(8,128)(2,1)S(1)} %slice.672), channel_id=1, source_target_pairs={{0,4},{4,8},{8,12},{12,16},{16,20},{20,24},{24,28},{28,32},{32,36}... | collective-permute-start | bytes 46088 | tf_op jit(solution)/shard_map/ppermute | solution.py:40
  216.4 7.4 %all-to-all-start.2 = ((f32[4,1,128]{2,1,0:T(1,128)}), f32[4,1,128]{2,1,0:T(1,128)S(1)}, u32[]{:S(2)}, u32[]{:S(2)}) async-start(f32[4,1,128]{2,1,0:T(1,128)} %broadcast_in_dim.27), calls=%async_computation.2 | async-start | bytes 4096 | tf_op jit(solution)/shard_map/all_to_all | solution.py:21
  225.6 22.2 %copy-start.6 = (f32[512]{0:T(512)S(1)}, f32[512]{0:T(512)}, u32[]{:S(2)}) copy-start(f32[512]{0:T(512)} %param.29) | copy-start | bytes 6148
  225.6 204.1 %all-to-all-start = ((bf16[128,16,768]{2,1,0:T(8,128)(2,1)}), bf16[128,16,768]{2,1,0:T(8,128)(2,1)}, u32[]{:S(2)}, u32[]{:S(2)}) async-start(bf16[128,16,768]{2,1,0:T(8,128)(2,1)} %stack.2), calls=%async_computation | async-start | bytes 6291456 | tf_op jit(solution)/shard_map/all_to_all | solution.py:79
  248.1 172.1 %copy-start.1 = (bf16[4,2,256,256]{3,2,1,0:T(8,128)(2,1)S(1)}, bf16[4,2,256,256]{3,2,1,0:T(8,128)(2,1)}, u32[]{:S(2)}) copy-start(bf16[4,2,256,256]{3,2,1,0:T(8,128)(2,1)} %all-gather.15.cloned.1.call-done) | copy-start | bytes 3145732
  424.9 9.8 %copy-start.7 = (f32[256]{0:T(256)S(1)}, f32[256]{0:T(256)}, u32[]{:S(2)}) copy-start(f32[256]{0:T(256)} %param.21) | copy-start | bytes 3076
  430.4 8.4 %all-to-all-start.4 = ((f32[4,1,128]{2,1,0:T(1,128)}), f32[4,1,128]{2,1,0:T(1,128)S(1)}, u32[]{:S(2)}, u32[]{:S(2)}) async-start(f32[4,1,128]{2,1,0:T(1,128)} %broadcast_in_dim.33), calls=%async_computation.4 | async-start | bytes 4096 | tf_op jit(solution)/shard_map/all_to_all | solution.py:21
Sparse Core Ops, SparseCore 0:
  10.9 152.9 all-gather.12
  172.2 24.0 all-gather.14
  198.7 142.0 all-gather.16
